TPU v7x, 32 devices: a whole 2x2x4 slice. The times are simulated.
32 devices in a mesh: sp: 4 (over z), fs: 4 (over y, x), tp: 2 (over core).
Axes of the slice: x: 2, y: 2, z: 4, core: 2. Of those that a mesh axis runs over, the one named last changes fastest.
Arguments:
- tokens: bfloat16 [2048, 2048], P(('fs', 'sp'), 'tp'), parts along dimension 0, may hold values from -6 to 6
- norm_gain: float32 [2048], replicated, may hold values from 0.1 to 1.9
- w_recur_in: bfloat16 [2048, 1024], P(None, 'tp'), may hold values from -0.125 to 0.125
- conv_weight: float32 [4, 1024], P(None, 'tp'), may hold values from -3 to 3
- w_gate_decay: bfloat16 [16, 64, 64], P('tp'), may hold values from -0.75 to 0.75
- w_gate_input: bfloat16 [16, 64, 64], P('tp'), may hold values from -0.75 to 0.75
- decay_base: float32 [1024], P('tp'), may hold values from 0 to 0.01, as said below
- extra_decay: float32 [2048, 16], P(('fs', 'sp'), 'tp'), parts along dimension 0, may hold values from 0 to 1, as said below
- w_query: bfloat16 [2048, 1024], P(None, 'tp'), may hold values from -1 to 1
- w_key: bfloat16 [2048, 256], P(None, 'tp'), may hold values from -20 to 20
- w_value: bfloat16 [2048, 256], P(None, 'tp'), may hold values from -0.125 to 0.125
- mix_lambda: float32 [8], P('tp'), may hold values from 0.3 to 0.8
- head_gain: float32 [128], replicated, may hold values from 0.1 to 1.9
- w_out_recur: bfloat16 [1024, 2048], P('tp'), may hold values from -0.125 to 0.125
- w_out_attend: bfloat16 [1024, 2048], P('tp'), may hold values from -0.125 to 0.125
- out_gain: float32 [2048], replicated, may hold values from 0.1 to 1.9
Outputs:
- mixed: bfloat16 [2048, 2048], P(('fs', 'sp', 'tp')), parts along dimension 0
There are 4 independent parts, one for each index of `fs`. A program takes and returns all parts, laid end to end along the dimension named above; an argument that names none is the same for every part. Nothing has to cross between parts.
Inputs may be any that keep to these rules, and one draw needn't show every extreme that they name: `decay_base`: positive rates of each channel. `extra_decay`: non-negative added log-decays.
All inputs are finite; a program needn't handle non-finite values.
Results may differ from a plain program's by a relative error of at most 0.012.
The roundings to bfloat16 on the way count: a program that leaves them out, or rounds other values in their place, can miss the bound.
Values may be sent and summed in bfloat16 or wider, within the bound.
A program may use at most 128 MiB of HBM per device.

v0:
```python
import jax
import jax.numpy as jnp
from jax import lax
from jax.sharding import PartitionSpec as P

D = 2048
HEAD = 64
DV = 128
lru_rate = 8.0
norm_eps = 1e-06


def shifted(block, axis, distance):
    devices = range(lax.axis_size(axis))
    route = [(i - distance, i) for i in devices if i - distance in devices]
    return lax.ppermute(block, axis, route)


def prefix(part, axis, combine, identity):
    place = lax.axis_index(axis)
    gathered = jax.tree.map(lambda a: lax.all_gather(a, axis), part)
    state = jax.tree.map(lambda a, e: jnp.zeros_like(a) + jnp.asarray(e, a.dtype), part, identity)

    def one(lap, state):
        return combine(
            state, jax.tree.map(lambda a: lax.dynamic_index_in_dim(a, lap, 0, False), gathered)
        )

    return lax.fori_loop(0, place, one, state)


def chain(earlier, later):
    return (earlier[0] * later[0], later[0] * earlier[1] + later[1])


def body(
    tokens,
    norm_gain,
    w_recur_in,
    conv_weight,
    w_gate_decay,
    w_gate_input,
    decay_base,
    extra_decay,
    w_query,
    w_key,
    w_value,
    mix_lambda,
    head_gain,
    w_out_recur,
    w_out_attend,
    out_gain,
):
    row_count = tokens.shape[0]
    recur_cols = w_recur_in.shape[1]
    query_cols = w_query.shape[1]
    key_cols = w_key.shape[1]
    all_weights = jnp.concatenate([w_recur_in, w_query, w_key, w_value], axis=1)
    wide_piece = lax.all_gather(tokens, "tp", axis=1, tiled=True).astype(jnp.float32)
    scaled = (wide_piece * norm_gain).astype(jnp.bfloat16)
    accum = jnp.dot(scaled, all_weights, preferred_element_type=jnp.float32)
    squares = jnp.sum(wide_piece * wide_piece, axis=1, keepdims=True)
    accum, squares = (accum, squares)
    inverse = lax.rsqrt(squares / D + norm_eps)
    projected = (accum * inverse).astype(jnp.bfloat16)
    recur_in = projected[:, :recur_cols]
    queries = projected[:, recur_cols : recur_cols + query_cols]
    keys = projected[:, recur_cols + query_cols : recur_cols + query_cols + key_cols]
    values = projected[:, recur_cols + query_cols + key_cols :]
    taps = conv_weight.shape[0]
    carried_rows = shifted(recur_in[row_count - (taps - 1) :], "sp", 1)
    padded = jnp.concatenate([carried_rows, recur_in], axis=0).astype(jnp.float32)
    conv_acc = jnp.zeros((row_count, recur_cols), jnp.float32)
    for offset in range(taps):
        conv_acc = conv_acc + conv_weight[offset] * padded[offset : offset + row_count]
    conv_in = conv_acc.astype(jnp.bfloat16)
    gate_blocks = w_gate_decay.shape[0]
    blocks = conv_in.reshape(row_count, gate_blocks, HEAD)
    decay_gate = jax.nn.sigmoid(
        jnp.einsum("thi,hij->thj", blocks, w_gate_decay, preferred_element_type=jnp.float32)
    ).reshape(row_count, recur_cols)
    input_gate = jax.nn.sigmoid(
        jnp.einsum("thi,hij->thj", blocks, w_gate_input, preferred_element_type=jnp.float32)
    ).reshape(row_count, recur_cols)
    log_decay = -lru_rate * decay_gate * decay_base - jnp.repeat(extra_decay, HEAD, axis=1)
    decay = jnp.exp(log_decay)
    inject = jnp.sqrt(-jnp.expm1(2.0 * log_decay)) * input_gate * conv_in.astype(jnp.float32)
    decay_cum, local_state = lax.associative_scan(chain, (decay, inject), axis=0)
    identity = (jnp.ones((recur_cols,), jnp.float32), jnp.zeros((recur_cols,), jnp.float32))
    carried = prefix((decay_cum[row_count - 1], local_state[row_count - 1]), "sp", chain, identity)
    recur_out = (local_state + decay_cum * carried[1]).astype(jnp.bfloat16)
    kv_local = key_cols // (2 * HEAD)
    heads_local = query_cols // (2 * HEAD)
    group_size = heads_local // kv_local
    local_query = queries.reshape(row_count, kv_local, group_size, 2, HEAD)
    offset_rows = lax.axis_index("sp") * row_count
    positions = offset_rows + jnp.arange(row_count, dtype=jnp.int32)
    last_position = offset_rows + row_count - 1
    lambdas = mix_lambda.reshape(kv_local, group_size)
    start_state = (
        jnp.full((2, kv_local, group_size, row_count), -1e30, jnp.float32),
        jnp.zeros((2, kv_local, group_size, row_count), jnp.float32),
        jnp.zeros((2, row_count, kv_local, group_size, DV), jnp.float32),
    )
    key_piece = lax.all_gather(keys, "sp", axis=0, tiled=True)
    value_piece = lax.all_gather(values, "sp", axis=0, tiled=True)
    count = key_piece.shape[0]

    def update(state):
        peaks, totals, attends = state
        key_three = key_piece.reshape(count, kv_local, 2, HEAD)
        value_three = value_piece.reshape(count, kv_local, DV)
        allowed = positions[:, None] >= jnp.arange(count, dtype=jnp.int32)[None, :]
        new_peaks, new_totals, new_attends = ([], [], [])
        for mapping in range(2):
            scores = jnp.einsum(
                "bkgd,tkd->kgbt",
                local_query[:, :, :, mapping, :],
                key_three[:, :, mapping, :],
                preferred_element_type=jnp.float32,
            ) * HEAD ** (-0.5)
            scores = jnp.where(allowed, scores, -jnp.inf)
            peak = jnp.maximum(peaks[mapping], jnp.max(scores, axis=-1))
            correction = jnp.exp(peaks[mapping] - peak)
            expo = jnp.exp(scores - peak[..., None])
            new_totals.append(totals[mapping] * correction + jnp.sum(expo, axis=-1))
            gained = jnp.einsum(
                "kgbt,tke->bkge",
                expo.astype(jnp.bfloat16),
                value_three,
                preferred_element_type=jnp.float32,
            )
            new_attends.append(
                attends[mapping] * jnp.transpose(correction, (2, 0, 1))[..., None] + gained
            )
            new_peaks.append(peak)
        return (jnp.stack(new_peaks), jnp.stack(new_totals), jnp.stack(new_attends))

    peaks, totals, attends = lax.cond(
        jnp.int32(0) <= last_position, update, lambda state: state, start_state
    )
    first = attends[0] / jnp.transpose(totals[0], (2, 0, 1))[..., None]
    second = attends[1] / jnp.transpose(totals[1], (2, 0, 1))[..., None]
    head_out = (first - lambdas[None, :, :, None] * second).reshape(row_count, heads_local, DV)
    normed = (
        head_out
        * lax.rsqrt(jnp.mean(head_out * head_out, axis=-1, keepdims=True) + norm_eps)
        * head_gain
    )
    attend_out = normed.astype(jnp.bfloat16).reshape(row_count, heads_local * DV)
    recur_rows, attend_rows = (
        lax.all_to_all(recur_out, "tp", split_axis=0, concat_axis=1, tiled=True),
        lax.all_to_all(attend_out, "tp", split_axis=0, concat_axis=1, tiled=True),
    )
    whole_recur, whole_attend = (
        lax.all_gather(w_out_recur, "tp", axis=0, tiled=True),
        lax.all_gather(w_out_attend, "tp", axis=0, tiled=True),
    )
    merged = jnp.dot(recur_rows, whole_recur, preferred_element_type=jnp.float32) + jnp.dot(
        attend_rows, whole_attend, preferred_element_type=jnp.float32
    )
    final = (
        merged * lax.rsqrt(jnp.mean(merged * merged, axis=1, keepdims=True) + norm_eps) * out_gain
    )
    return final.astype(jnp.bfloat16)


def solution(mesh):
    in_specs = (
        P(("fs", "sp"), "tp"),
        P(),
        P(None, "tp"),
        P(None, "tp"),
        P("tp", None, None),
        P("tp", None, None),
        P("tp"),
        P(("fs", "sp"), "tp"),
        P(None, "tp"),
        P(None, "tp"),
        P(None, "tp"),
        P("tp"),
        P(),
        P("tp", None),
        P("tp", None),
        P(),
    )
    out_specs = P(("fs", "sp", "tp"), None)
    return jax.shard_map(body, mesh=mesh, in_specs=in_specs, out_specs=out_specs, check_vma=False)
```

profile of v0, /device:TPU:0, one launch (start us, length us, event | category | flops | bytes accessed | tf_op | source)
XLA Modules:
  0.0 101.6 jit_solution(12139623973826426824)
XLA Ops:
  6.5 0.7 all-gather.5.cloned.1.call-update
  7.3 2.5 %all_gather.21 = bf16[128,2048]{1,0:T(8,128)(2,1)S(1)} all-gather(bf16[128,1024]{1,0:T(8,128)(2,1)} %param.20), channel_id=1, replica_groups=mesh['sp'=4,'fs'=4,'tp'=2] {'tp'}, dimensions={1}, use_global_device_ids=true | all-gather | bytes 786432 | tf_op jit(solution)/shard_map/all_gather | solution.py:59
  9.8 0.2 fusion.43
  10.0 3.2 %fusion.33 = bf16[128,1280]{1,0:T(8,128)(2,1)S(1)} fusion(bf16[2048,128]{1,0:T(8,128)(2,1)} %param.30, bf16[2048,128]{1,0:T(8,128)(2,1)} %param.29, bf16[2048,512]{1,0:T(8,128)(2,1)} %param.28, bf16[2048,512]{1,0:T(8,128)(2,1)} %param.22, bf16[128,2048]{1,0:T(8,128)(2,1)S(1)} %all_gather.21, f32[2048]{0:T(1024)} %param.21, f32[128]{0:T(128)S(1)} %add_rsqrt_fusion.2), kind=kOutput, calls=%fused_computation.52 | convolution fusion | flops 693174272 | bytes 6103552 | tf_op jit(solution)/shard_map/dot_general | solution.py:61
  13.2 4.8 %collective-permute-start = (bf16[3,512]{1,0:T(4,128)(2,1)S(1)}, bf16[3,512]{1,0:T(4,128)(2,1)S(1)}, u32[]{:S(2)}, u32[]{:S(2)}) collective-permute-start(bf16[3,512]{1,0:T(4,128)(2,1)S(1)} %slice.358), channel_id=1, source_target_pairs={{0,8},{8,16},{16,24},{1,9},{9,17},{17,25},{2,10},{10,18},{18,26},{... | collective-permute-start | bytes 9224 | tf_op jit(solution)/shard_map/ppermute | solution.py:16
  18.0 13.6 %all_gather.25 = bf16[512,128]{1,0:T(8,128)(2,1)S(1)} all-gather(bf16[128,128]{1,0:T(8,128)(2,1)S(1)} %get-tuple-element.115), channel_id=1, replica_groups=mesh['sp'=4,'fs'=4,'tp'=2] {'sp'}, dimensions={0}, use_global_device_ids=true | all-gather | bytes 163840 | tf_op jit(solution)/shard_map/all_gather | solution.py:105
  31.6 13.4 %all_gather.26 = bf16[512,128]{1,0:T(8,128)(2,1)S(1)} all-gather(bf16[128,128]{1,0:T(8,128)(2,1)S(1)} %get-tuple-element.114), channel_id=1, replica_groups=mesh['sp'=4,'fs'=4,'tp'=2] {'sp'}, dimensions={0}, use_global_device_ids=true | all-gather | bytes 163840 | tf_op jit(solution)/shard_map/all_gather | solution.py:106
  45.0 2.2 %conditional.1 = (f32[2,1,4,128]{3,2,1,0:T(4,128)S(1)}, f32[2,128,1,4,128]{4,1,3,2,0:T(8,128)S(1)}) conditional(s32[]{:T(128)} %convert_element_type.45, () %tuple.21, (s32[]{:T(128)}, s32[128]{0:T(128)S(1)}, bf16[512,128]{1,0:T(8,128)(2,1)S(1)}, bf16[128,1280]{1,0:T(8,128)(2,1)S(1)}, bf16[512,128]{1,0:T(8,128)(2,1)S(1)}) %tuple.22), branch_computations={%region_3.4_spmd, %region_4.9_spmd} | conditional | flops 205328512 | bytes 9819668 | solution.py:139
  45.0 0.2 copy.57
  45.3 0.1 copy.56
  45.4 0.3 fusion.65
  45.8 0.2 fusion.11
  46.0 0.3 fusion.66
  46.3 0.2 fusion.9
  46.5 0.4 fusion.5
  46.9 0.4 fusion.7
  47.3 0.0 copy-start.6
  47.3 0.1 copy.72
  47.4 0.1 copy.73
  47.5 0.3 fusion.53
  47.9 0.1 copy.62
  48.0 0.2 mul.337
  48.2 0.1 mul.338
  48.3 0.0 copy-start.2
  48.3 0.0 copy-start.5
  48.4 0.2 copy.58
  48.6 0.1 squeeze.135
  48.7 0.2 copy.60
  48.9 0.1 squeeze.137
  49.0 0.2 div.75.clone
  49.2 0.1 div.76
  49.3 0.2 div.79.clone
  49.5 0.1 div.80
  49.6 0.1 broadcast_bitcast_fusion
  49.7 0.8 multiply_convert_fusion.1
  50.5 3.4 %all-to-all-start.1 = ((bf16[2,64,512]{2,1,0:T(8,128)(2,1)}), bf16[2,64,512]{2,1,0:T(8,128)(2,1)S(1)}, u32[]{:S(2)}, u32[]{:S(2)}) async-start(bf16[2,64,512]{2,1,0:T(8,128)(2,1)} %multiply_convert_fusion.1), calls=%async_computation.1 | async-start | bytes 262144 | tf_op jit(solution)/shard_map/all_to_all | solution.py:153
  53.8 0.0 all-gather.7.cloned.1.call-start
  53.9 0.7 all-gather.7.cloned.1.call-update
  54.7 0.1 copy.52
  54.8 0.5 all-to-all-done.1
  55.4 0.1 fusion.47
  55.5 0.1 copy.49
  55.6 0.3 fusion.41
  55.9 0.1 copy.51
  56.0 0.3 fusion.38
  56.3 0.1 copy.54
  56.5 0.3 convert_multiply_fusion.2
  56.8 0.1 slice.284
  56.9 0.1 slice.285
  57.0 0.1 slice.283
  57.1 0.1 slice.287
  58.2 0.2 slice.282
  58.4 0.2 slice.331
  59.5 0.1 fusion.54
  59.6 11.9 %all-gather.1 = f32[4,1,512]{2,1,0:T(1,128)S(1)} all-gather(f32[1,1,512]{2,1,0:T(1,128)S(1)} %add_bitcast_fusion.2), channel_id=1, replica_groups=mesh['sp'=4,'fs'=4,'tp'=2] {'sp'}, dimensions={0}, use_global_device_ids=true | all-gather | bytes 10240 | tf_op jit(solution)/shard_map/all_gather | solution.py:21
  71.7 11.9 %all-gather = f32[4,1,512]{2,1,0:T(1,128)S(1)} all-gather(f32[1,1,512]{2,1,0:T(1,128)S(1)} %add_bitcast_fusion.3), channel_id=1, replica_groups=mesh['sp'=4,'fs'=4,'tp'=2] {'sp'}, dimensions={0}, use_global_device_ids=true | all-gather | bytes 10240 | tf_op jit(solution)/shard_map/all_gather | solution.py:21
  83.6 0.1 add_convert_fusion
  83.8 3.8 %all_to_all.35 = bf16[2,64,512]{2,1,0:T(8,128)(2,1)S(1)} all-to-all(bf16[2,64,512]{2,1,0:T(8,128)(2,1)S(1)} %bitcast.174), channel_id=1, replica_groups=mesh['sp'=4,'fs'=4,'tp'=2] {'tp'}, dimensions={0} | all-to-all | bytes 262144 | tf_op jit(solution)/shard_map/all_to_all | solution.py:152
  87.6 0.0 all-gather.5.cloned.1.call-done
  87.6 0.0 copy-start.1
  87.6 3.0 %fusion.71 = f32[64,2048]{1,0:T(8,128)S(1)} fusion(bf16[64,1024]{1,0:T(8,128)(2,1)S(1)} %bitcast.175, bf16[1024,2048]{1,0:T(8,128)(2,1)} %all-gather.5.cloned.1.call-done), kind=kOutput, calls=%fused_computation.154 | convolution fusion | flops 268435456 | bytes 4849664 | tf_op jit(solution)/shard_map/dot_general | solution.py:159
  90.7 0.0 all-gather.7.cloned.1.call-done
  90.7 3.2 %multiply_reduce_fusion = (f32[64]{0:T(128)S(1)}, f32[64,2048]{1,0:T(8,128)S(1)}) fusion(f32[64,2048]{1,0:T(8,128)S(1)} %fusion.71, bf16[64,1024]{1,0:T(8,128)(2,1)S(1)} %bitcast.173, bf16[1024,2048]{1,0:T(8,128)(2,1)} %all-gather.7.cloned.1.call-done), kind=kOutput, calls=%fused_computation.67 | convolution fusion | flops 268828608 | bytes 5374208 | tf_op jit(solution)/shard_map/dot_general | solution.py:159
  93.9 0.8 multiply_convert_fusion
  (139 shorter events, 1.9 us)
Async XLA Ops:
  6.5 49.1 %copy-start = (bf16[8,64,64]{2,1,0:T(8,128)(2,1)S(1)}, bf16[8,64,64]{2,1,0:T(8,128)(2,1)}, u32[]{:S(2)}) copy-start(bf16[8,64,64]{2,1,0:T(8,128)(2,1)} %param.24) | copy-start | bytes 196612
  6.5 81.1 %all-gather.5.cloned.1.call-start = ((), (), s32[]{:S(2)}) async-start(), calls=%async_computation.2 | async-start | bytes 6291456 | tf_op jit(solution)/shard_map/all_gather | solution.py:156
  13.2 42.1 %collective-permute-start = (bf16[3,512]{1,0:T(4,128)(2,1)S(1)}, bf16[3,512]{1,0:T(4,128)(2,1)S(1)}, u32[]{:S(2)}, u32[]{:S(2)}) collective-permute-start(bf16[3,512]{1,0:T(4,128)(2,1)S(1)} %slice.358), channel_id=1, source_target_pairs={{0,8},{8,16},{16,24},{1,9},{9,17},{17,25},{2,10},{10,18},{18,26},{... | collective-permute-start | bytes 9224 | tf_op jit(solution)/shard_map/ppermute | solution.py:16
  45.0 2.5 %copy-start.4 = (f32[4]{0:T(128)S(1)}, f32[4]{0:T(128)}, u32[]{:S(2)}) copy-start(f32[4]{0:T(128)} %param.31) | copy-start | bytes 52
  47.3 2.3 %copy-start.6 = (f32[128]{0:T(128)S(1)}, f32[128]{0:T(128)}, u32[]{:S(2)}) copy-start(f32[128]{0:T(128)} %param.32) | copy-start | bytes 1540
  48.3 6.3 %copy-start.2 = (f32[4,512]{1,0:T(4,128)S(1)}, f32[4,512]{1,0:T(4,128)}, u32[]{:S(2)}) copy-start(f32[4,512]{1,0:T(4,128)} %param.23) | copy-start | bytes 24580
  48.3 6.3 %copy-start.5 = (f32[512]{0:T(512)S(1)}, f32[512]{0:T(512)}, u32[]{:S(2)}) copy-start(f32[512]{0:T(512)} %param.26) | copy-start | bytes 6148
  48.4 6.3 %copy-start.3 = (f32[128,8]{0,1:T(8,128)S(1)}, f32[128,8]{0,1:T(8,128)}, u32[]{:S(2)}) copy-start(f32[128,8]{0,1:T(8,128)} %param.27) | copy-start | bytes 12292
  49.7 6.4 %copy-start.7 = (bf16[8,64,64]{2,1,0:T(8,128)(2,1)S(1)}, bf16[8,64,64]{2,1,0:T(8,128)(2,1)}, u32[]{:S(2)}) copy-start(bf16[8,64,64]{2,1,0:T(8,128)(2,1)} %param.25) | copy-start | bytes 196612
  50.5 4.8 %all-to-all-start.1 = ((bf16[2,64,512]{2,1,0:T(8,128)(2,1)}), bf16[2,64,512]{2,1,0:T(8,128)(2,1)S(1)}, u32[]{:S(2)}, u32[]{:S(2)}) async-start(bf16[2,64,512]{2,1,0:T(8,128)(2,1)} %multiply_convert_fusion.1), calls=%async_computation.1 | async-start | bytes 262144 | tf_op jit(solution)/shard_map/all_to_all | solution.py:153
  53.8 36.9 %all-gather.7.cloned.1.call-start = ((), (), s32[]{:S(2)}) async-start(), calls=%async_computation.3 | async-start | bytes 6291456 | tf_op jit(solution)/shard_map/all_gather | solution.py:157
  87.6 6.3 %copy-start.1 = (f32[2048]{0:T(1024)S(1)}, f32[2048]{0:T(1024)}, u32[]{:S(2)}) copy-start(f32[2048]{0:T(1024)} %param.35) | copy-start | bytes 24580
Sparse Core Ops, SparseCore 0:
  8.9 16.3 all-gather.4
  56.2 12.8 all-gather.6
where the time goes:
time: 102 us
  blocking collectives  57.2 us (56%)
  between operations  14.4 us (14%)
  matrix products  11.3 us (11%)
  starting transfers between devices  8.26 us (8%)
  local copies, waits for them, and re-layouts  4.75 us (5%)
  other arithmetic  3.69 us (4%)
  waiting for transfers between devices  1.91 us (2%)
    all_gather x2, blocking collectives, prefix(): gathered = jax.tree.map(lambda a: lax.all_gather(a, axis), part)  23.9 us
    all_gather x1, blocking collectives, body(): key_piece = lax.all_gather(keys, 'sp', axis=0, tiled=True)  13.6 us
    all_gather x1, blocking collectives, body(): value_piece = lax.all_gather(values, 'sp', axis=0, tiled=True)  13.4 us
    ppermute x1, starting transfers between devices, shifted(): return lax.ppermute(block, axis, route)  4.84 us
    all_to_all x1, blocking collectives, body(): lax.all_to_all(recur_out, 'tp', split_axis=0, concat_axis=1, tiled=True)  3.84 us
    all_to_all x1, starting transfers between devices, body(): lax.all_to_all(attend_out, 'tp', split_axis=0, concat_axis=1, tiled=True)  3.38 us
    dot_general x1, matrix products, body(): accum = jnp.dot(scaled, all_weights, preferred_element_type=jnp.float32)  3.19 us
    dot_general x1, matrix products, body(): jnp.dot(attend_rows, whole_attend, preferred_element_type=jnp.float32)  3.16 us
  transfers between devices with their start and end apart: 4, of which 1 were waited for; matrix products, arithmetic and copies ran while one was open for 15% of the time, Pallas kernels for 0%

commit v1 on v0

--- a/solution.py
+++ b/solution.py
@@ -103,7 +103,16 @@
         jnp.zeros((2, row_count, kv_local, group_size, DV), jnp.float32),
     )
     key_piece = lax.all_gather(keys, "sp", axis=0, tiled=True)
-    value_piece = lax.all_gather(values, "sp", axis=0, tiled=True)
+    cores_n = lax.axis_size("sp")
+    ledger = tuple(((dev_j, (dev_j + 1) % cores_n) for dev_j in range(cores_n)))
+    r2 = [None] * cores_n
+    r2[cores_n - 1] = values
+    for b in range(cores_n - 2, -1, -1):
+        r2[b] = lax.ppermute(r2[b + 1], "sp", perm=ledger)
+    m_next = jnp.concatenate(r2, 0)
+    z_new = lax.axis_index("sp")
+    z2 = (z_new + 1) * values.shape[0]
+    value_piece = jnp.roll(m_next, z2, 0)
     count = key_piece.shape[0]
 
     def update(state):

time: 102 us -> 97.9 us (0.960)
  blocking collectives: 57.2 us -> 48.3 us
  waiting for transfers between devices: 1.91 us -> 9.16 us
  starting transfers between devices: 8.26 us -> 6.55 us
    all_gather x1 -> x0, blocking collectives: 13.4 us -> none  [body(): value_piece = lax.all_gather(values, 'sp', axis=0, tiled=True)]
    ppermute x0 -> x3, waiting for transfers between devices: none -> 7.42 us  [body(): r2[b] = lax.ppermute(r2[b + 1], 'sp', perm=ledger)]
    all_to_all x0 -> x1, blocking collectives: none -> 3.84 us  [body(): lax.all_to_all(attend_out, 'tp', split_axis=0, concat_axis=1, tiled=True)]
    all_to_all x1 -> x0, starting transfers between devices: 3.38 us -> none  [body(): lax.all_to_all(attend_out, 'tp', split_axis=0, concat_axis=1, tiled=True)]
    ppermute x0 -> x3, starting transfers between devices: none -> 3.04 us  [body(): r2[b] = lax.ppermute(r2[b + 1], 'sp', perm=ledger)]
    ppermute x1, starting transfers between devices: 4.84 us -> 3.47 us  [shifted(): return lax.ppermute(block, axis, route)]
  transfers between devices with their start and end apart: 4 -> 6, of which waited for: 1 -> 3; matrix products, arithmetic and copies ran while one was open for 15% -> 15% of each run, Pallas kernels for 0% -> 0%
where the time goes in v1:
time: 97.9 us; the launch traced here: 97.6 us
  blocking collectives  48.3 us (49%)
  between operations  14.4 us (15%)
  matrix products  11.3 us (12%)
  waiting for transfers between devices  9.16 us (9%)
  starting transfers between devices  6.55 us (7%)
  local copies, waits for them, and re-layouts  4.94 us (5%)
  other arithmetic  2.85 us (3%)
    all_gather x2, blocking collectives, prefix(): gathered = jax.tree.map(lambda a: lax.all_gather(a, axis), part)  24.8 us
    all_gather x1, blocking collectives, body(): key_piece = lax.all_gather(keys, 'sp', axis=0, tiled=True)  13.3 us
    ppermute x3, waiting for transfers between devices, body(): r2[b] = lax.ppermute(r2[b + 1], 'sp', perm=ledger)  7.42 us
    all_to_all x1, blocking collectives, body(): lax.all_to_all(recur_out, 'tp', split_axis=0, concat_axis=1, tiled=True)  3.84 us
    all_to_all x1, blocking collectives, body(): lax.all_to_all(attend_out, 'tp', split_axis=0, concat_axis=1, tiled=True)  3.84 us
    ppermute x1, starting transfers between devices, shifted(): return lax.ppermute(block, axis, route)  3.47 us
    dot_general x1, matrix products, body(): accum = jnp.dot(scaled, all_weights, preferred_element_type=jnp.float32)  3.19 us
    dot_general x1, matrix products, body(): jnp.dot(attend_rows, whole_attend, preferred_element_type=jnp.float32)  3.16 us
  transfers between devices with their start and end apart: 6, of which 3 were waited for; matrix products, arithmetic and copies ran while one was open for 15% of the time, Pallas kernels for 0%

profile of v1, /device:TPU:0, one launch (start us, length us, event | category | flops | bytes accessed | tf_op | source)
XLA Modules:
  0.0 97.6 jit_solution(2115988486065965241)
XLA Ops:
  6.5 0.7 all-gather.5.cloned.1.call-update
  7.3 0.0 all-gather.7.cloned.1.call-start
  7.3 2.5 %all_gather.18 = bf16[128,2048]{1,0:T(8,128)(2,1)S(1)} all-gather(bf16[128,1024]{1,0:T(8,128)(2,1)} %param.20), channel_id=1, replica_groups=mesh['sp'=4,'fs'=4,'tp'=2] {'tp'}, dimensions={1}, use_global_device_ids=true | all-gather | bytes 786432 | tf_op jit(solution)/shard_map/all_gather | solution.py:59
  9.8 0.2 fusion.47
  10.1 3.2 %fusion.37 = bf16[128,1280]{1,0:T(8,128)(2,1)S(1)} fusion(bf16[2048,128]{1,0:T(8,128)(2,1)} %param.30, bf16[2048,128]{1,0:T(8,128)(2,1)} %param.29, bf16[2048,512]{1,0:T(8,128)(2,1)} %param.28, bf16[2048,512]{1,0:T(8,128)(2,1)} %param.22, bf16[128,2048]{1,0:T(8,128)(2,1)S(1)} %all_gather.18, f32[2048]{0:T(1024)} %param.21, f32[128]{0:T(128)S(1)} %add_rsqrt_fusion.2), kind=kOutput, calls=%fused_computation.56 | convolution fusion | flops 693174272 | bytes 6103552 | tf_op jit(solution)/shard_map/dot_general | solution.py:61
  13.3 3.0 %collective-permute-start.1 = (bf16[128,128]{1,0:T(8,128)(2,1)S(1)}, bf16[128,128]{1,0:T(8,128)(2,1)S(1)}, u32[]{:S(2)}, u32[]{:S(2)}) collective-permute-start(bf16[128,128]{1,0:T(8,128)(2,1)S(1)} %slice.431), channel_id=1, source_target_pairs={{0,8},{8,16},{16,24},{24,0},{1,9},{9,17},{17,25},{25,1},{2,10},{10... | collective-permute-start | bytes 98312 | tf_op jit(solution)/shard_map/ppermute | solution.py:111
  16.3 3.5 %collective-permute-start = (bf16[3,512]{1,0:T(4,128)(2,1)S(1)}, bf16[3,512]{1,0:T(4,128)(2,1)S(1)}, u32[]{:S(2)}, u32[]{:S(2)}) collective-permute-start(bf16[3,512]{1,0:T(4,128)(2,1)S(1)} %slice.378), channel_id=1, source_target_pairs={{0,8},{8,16},{16,24},{1,9},{9,17},{17,25},{2,10},{10,18},{18,26},{... | collective-permute-start | bytes 9224 | tf_op jit(solution)/shard_map/ppermute | solution.py:16
  19.8 0.0 all-gather.7.cloned.1.call-update
  19.8 0.1 broadcast_bitcast_fusion
  20.0 0.1 copy.54
  20.1 1.0 collective-permute-done
  21.1 0.1 fusion.51
  21.2 0.1 copy.51
  21.4 0.3 fusion.45
  21.7 0.1 copy.53
  21.8 0.3 fusion.42
  22.1 0.1 copy.56
  22.2 0.3 convert_multiply_fusion.2
  22.6 0.1 slice.299
  22.7 0.1 slice.300
  22.8 0.1 slice.298
  22.9 0.1 slice.302
  23.9 0.2 slice.297
  24.1 0.2 slice.346
  25.2 0.1 fusion.58
  25.5 12.9 %all-gather.1 = f32[4,1,512]{2,1,0:T(1,128)S(1)} all-gather(f32[1,1,512]{2,1,0:T(1,128)S(1)} %add_bitcast_fusion.2), channel_id=1, replica_groups=mesh['sp'=4,'fs'=4,'tp'=2] {'sp'}, dimensions={0}, use_global_device_ids=true | all-gather | bytes 10240 | tf_op jit(solution)/shard_map/all_gather | solution.py:21
  38.4 11.9 %all-gather = f32[4,1,512]{2,1,0:T(1,128)S(1)} all-gather(f32[1,1,512]{2,1,0:T(1,128)S(1)} %add_bitcast_fusion.3), channel_id=1, replica_groups=mesh['sp'=4,'fs'=4,'tp'=2] {'sp'}, dimensions={0}, use_global_device_ids=true | all-gather | bytes 10240 | tf_op jit(solution)/shard_map/all_gather | solution.py:21
  50.3 0.1 collective-permute-start.2
  50.4 5.7 %collective-permute-done.2 = bf16[128,128]{1,0:T(8,128)(2,1)S(1)} collective-permute-done((bf16[128,128]{1,0:T(8,128)(2,1)S(1)}, bf16[128,128]{1,0:T(8,128)(2,1)S(1)}, u32[]{:S(2)}, u32[]{:S(2)}) %collective-permute-start.2) | collective-permute-done | bytes 32800 | tf_op jit(solution)/shard_map/ppermute | solution.py:111
  56.1 0.1 add_convert_fusion
  56.2 3.8 %all_to_all.35 = bf16[2,64,512]{2,1,0:T(8,128)(2,1)S(1)} all-to-all(bf16[2,64,512]{2,1,0:T(8,128)(2,1)S(1)} %bitcast.171), channel_id=1, replica_groups=mesh['sp'=4,'fs'=4,'tp'=2] {'tp'}, dimensions={0} | all-to-all | bytes 262144 | tf_op jit(solution)/shard_map/all_to_all | solution.py:161
  60.0 1.7 %collective-permute-done.3 = bf16[128,128]{1,0:T(8,128)(2,1)S(1)} collective-permute-done((bf16[128,128]{1,0:T(8,128)(2,1)S(1)}, bf16[128,128]{1,0:T(8,128)(2,1)S(1)}, u32[]{:S(2)}, u32[]{:S(2)}) %collective-permute-start.3) | collective-permute-done | bytes 32800 | tf_op jit(solution)/shard_map/ppermute | solution.py:111
  61.9 13.3 %all_gather.22 = bf16[512,128]{1,0:T(8,128)(2,1)S(1)} all-gather(bf16[128,128]{1,0:T(8,128)(2,1)S(1)} %get-tuple-element.246), channel_id=1, replica_groups=mesh['sp'=4,'fs'=4,'tp'=2] {'sp'}, dimensions={0}, use_global_device_ids=true | all-gather | bytes 163840 | tf_op jit(solution)/shard_map/all_gather | solution.py:105
  75.2 2.4 %conditional.1 = (f32[2,1,4,128]{3,2,1,0:T(4,128)S(1)}, f32[2,128,1,4,128]{1,4,3,2,0:T(8,128)S(1)}) conditional(s32[]{:T(128)} %convert_element_type.51, () %tuple.32, (s32[]{:T(128)}, s32[128]{0:T(128)S(1)}, bf16[512,128]{1,0:T(8,128)(2,1)S(1)}, bf16[128,1280]{1,0:T(8,128)(2,1)S(1)}, s32[]{:T(128)}, /*index=5*/s32[]{:T(128)}, ...), branch_computations={%region_3.4_spmd, %region_4.9_spmd.clone} | conditional | flops 205328512 | bytes 10344119 | solution.py:148
  75.2 0.2 copy.59
  75.5 0.1 copy.58
  75.7 0.3 fusion.69
  76.0 0.2 fusion.11
  76.2 0.3 fusion.70
  76.5 0.2 fusion.9
  76.7 0.1 copy.60
  76.9 0.3 fusion.5
  77.2 0.3 fusion.7
  77.6 0.1 copy.75
  77.7 0.1 copy.76
  77.8 0.1 fusion.57
  78.0 0.1 copy.65
  78.1 0.2 mul.347
  78.3 0.1 mul.348
  78.5 0.1 copy.61
  78.6 0.1 squeeze.165
  78.7 0.1 copy.63
  78.9 0.1 squeeze.167
  79.0 0.2 div.75.clone
  79.2 0.1 div.76
  79.3 0.2 div.79.clone
  79.5 0.1 div.80
  79.6 0.1 multiply_convert_fusion.1
  79.8 3.8 %all_to_all.36 = bf16[2,64,512]{2,1,0:T(8,128)(2,1)S(1)} all-to-all(bf16[2,64,512]{2,1,0:T(8,128)(2,1)S(1)} %multiply_convert_fusion.1), channel_id=1, replica_groups=mesh['sp'=4,'fs'=4,'tp'=2] {'tp'}, dimensions={0} | all-to-all | bytes 262144 | tf_op jit(solution)/shard_map/all_to_all | solution.py:162
  83.6 0.0 all-gather.5.cloned.1.call-done
  83.7 3.0 %fusion.74 = f32[64,2048]{1,0:T(8,128)S(1)} fusion(bf16[64,1024]{1,0:T(8,128)(2,1)S(1)} %bitcast.169, bf16[1024,2048]{1,0:T(8,128)(2,1)} %all-gather.5.cloned.1.call-done), kind=kOutput, calls=%fused_computation.165 | convolution fusion | flops 268435456 | bytes 4849664 | tf_op jit(solution)/shard_map/dot_general | solution.py:168
  86.7 0.0 all-gather.7.cloned.1.call-done
  86.7 3.2 %multiply_reduce_fusion = (f32[64]{0:T(128)S(1)}, f32[64,2048]{1,0:T(8,128)S(1)}) fusion(f32[64,2048]{1,0:T(8,128)S(1)} %fusion.74, bf16[64,1024]{1,0:T(8,128)(2,1)S(1)} %bitcast.170, bf16[1024,2048]{1,0:T(8,128)(2,1)} %all-gather.7.cloned.1.call-done), kind=kOutput, calls=%fused_computation.71 | convolution fusion | flops 268828608 | bytes 5374208 | tf_op jit(solution)/shard_map/dot_general | solution.py:168
  89.9 0.8 multiply_convert_fusion
  (152 shorter events, 2.0 us)
Async XLA Ops:
  6.5 14.8 %copy-start = (bf16[8,64,64]{2,1,0:T(8,128)(2,1)S(1)}, bf16[8,64,64]{2,1,0:T(8,128)(2,1)}, u32[]{:S(2)}) copy-start(bf16[8,64,64]{2,1,0:T(8,128)(2,1)} %param.24) | copy-start | bytes 196612
  6.5 77.1 %all-gather.5.cloned.1.call-start = ((), (), s32[]{:S(2)}) async-start(), calls=%async_computation.2 | async-start | bytes 6291456 | tf_op jit(solution)/shard_map/all_gather | solution.py:165
  7.3 79.5 %all-gather.7.cloned.1.call-start = ((), (), s32[]{:S(2)}) async-start(), calls=%async_computation.3 | async-start | bytes 6291456 | tf_op jit(solution)/shard_map/all_gather | solution.py:166
  10.0 9.8 %copy-start.2 = (f32[4,512]{1,0:T(4,128)S(1)}, f32[4,512]{1,0:T(4,128)}, u32[]{:S(2)}) copy-start(f32[4,512]{1,0:T(4,128)} %param.23) | copy-start | bytes 24580
  10.0 9.8 %copy-start.4 = (f32[4]{0:T(128)S(1)}, f32[4]{0:T(128)}, u32[]{:S(2)}) copy-start(f32[4]{0:T(128)} %param.31) | copy-start | bytes 52
  10.0 9.8 %copy-start.6 = (f32[128]{0:T(128)S(1)}, f32[128]{0:T(128)}, u32[]{:S(2)}) copy-start(f32[128]{0:T(128)} %param.32) | copy-start | bytes 1540
  10.0 9.9 %copy-start.5 = (f32[512]{0:T(512)S(1)}, f32[512]{0:T(512)}, u32[]{:S(2)}) copy-start(f32[512]{0:T(512)} %param.26) | copy-start | bytes 6148
  10.1 9.9 %copy-start.3 = (f32[128,8]{0,1:T(8,128)S(1)}, f32[128,8]{0,1:T(8,128)}, u32[]{:S(2)}) copy-start(f32[128,8]{0,1:T(8,128)} %param.27) | copy-start | bytes 12292
  13.3 8.5 %copy-start.7 = (bf16[8,64,64]{2,1,0:T(8,128)(2,1)S(1)}, bf16[8,64,64]{2,1,0:T(8,128)(2,1)}, u32[]{:S(2)}) copy-start(bf16[8,64,64]{2,1,0:T(8,128)(2,1)} %param.25) | copy-start | bytes 196612
  13.3 37.0 %collective-permute-start.1 = (bf16[128,128]{1,0:T(8,128)(2,1)S(1)}, bf16[128,128]{1,0:T(8,128)(2,1)S(1)}, u32[]{:S(2)}, u32[]{:S(2)}) collective-permute-start(bf16[128,128]{1,0:T(8,128)(2,1)S(1)} %slice.431), channel_id=1, source_target_pairs={{0,8},{8,16},{16,24},{24,0},{1,9},{9,17},{17,25},{25,1},{2,10},{10... | collective-permute-start | bytes 98312 | tf_op jit(solution)/shard_map/ppermute | solution.py:111
  16.3 4.8 %collective-permute-start = (bf16[3,512]{1,0:T(4,128)(2,1)S(1)}, bf16[3,512]{1,0:T(4,128)(2,1)S(1)}, u32[]{:S(2)}, u32[]{:S(2)}) collective-permute-start(bf16[3,512]{1,0:T(4,128)(2,1)S(1)} %slice.378), channel_id=1, source_target_pairs={{0,8},{8,16},{16,24},{1,9},{9,17},{17,25},{2,10},{10,18},{18,26},{... | collective-permute-start | bytes 9224 | tf_op jit(solution)/shard_map/ppermute | solution.py:16
  50.3 5.8 %collective-permute-start.2 = (bf16[128,128]{1,0:T(8,128)(2,1)S(1)}, bf16[128,128]{1,0:T(8,128)(2,1)S(1)}, u32[]{:S(2)}, u32[]{:S(2)}) collective-permute-start(bf16[128,128]{1,0:T(8,128)(2,1)S(1)} %collective-permute-done.1), channel_id=1, source_target_pairs={{0,8},{8,16},{16,24},{24,0},{1,9},{9,17},{17,25},{25,1},{2,10},{10... | collective-permute-start | bytes 98312 | tf_op jit(solution)/shard_map/ppermute | solution.py:111
  56.1 5.7 %collective-permute-start.3 = (bf16[128,128]{1,0:T(8,128)(2,1)S(1)}, bf16[128,128]{1,0:T(8,128)(2,1)S(1)}, u32[]{:S(2)}, u32[]{:S(2)}) collective-permute-start(bf16[128,128]{1,0:T(8,128)(2,1)S(1)} %collective-permute-done.2), channel_id=1, source_target_pairs={{0,8},{8,16},{16,24},{24,0},{1,9},{9,17},{17,25},{25,1},{2,10},{10... | collective-permute-start | bytes 98312 | tf_op jit(solution)/shard_map/ppermute | solution.py:111
  83.7 6.3 %copy-start.1 = (f32[2048]{0:T(1024)S(1)}, f32[2048]{0:T(1024)}, u32[]{:S(2)}) copy-start(f32[2048]{0:T(1024)} %param.35) | copy-start | bytes 24580
Sparse Core Ops, SparseCore 0:
  8.9 16.3 all-gather.4
  26.8 14.8 all-gather.6
